TPU v7x, 32 devices: a whole 2x2x4 slice. The times are simulated.
32 devices in a mesh: grp: 2 (over x), ep: 8 (over z, y), tp: 2 (over core).
Axes of the slice: x: 2, y: 2, z: 4, core: 2. Of those that a mesh axis runs over, the one named last changes fastest.
Arguments:
- tokens: bfloat16 [1024, 2048], P(('grp', 'ep')), parts along dimension 0, may hold values from -6 to 6
- norm_gain: bfloat16 [2048], replicated, may hold values from 0.099609375 to 1.8984375
- routes: int32 [1024, 4], P(('grp', 'ep')), parts along dimension 0, may hold values from 0 to 7, all different within a row; in each aligned block of 64 rows (0 to 63, 64 to 127, ...) at most 64 rows name the same one
- route_weights: float32 [1024, 4], P(('grp', 'ep')), parts along dimension 0, may hold values from 0.2 to 1
- gate_experts: bfloat16 [8, 2048, 512], P('ep', None, 'tp'), may hold values from -0.125 to 0.125
- up_experts: bfloat16 [8, 2048, 512], P('ep', None, 'tp'), may hold values from -0.125 to 0.125
- down_experts: bfloat16 [8, 512, 2048], P('ep', 'tp'), may hold values from -0.25 to 0.25
- shared_gate: bfloat16 [2048, 512], P(None, 'tp'), may hold values from -0.125 to 0.125
- shared_up: bfloat16 [2048, 512], P(None, 'tp'), may hold values from -0.125 to 0.125
- shared_down: bfloat16 [512, 2048], P('tp'), may hold values from -0.25 to 0.25
- out_gain: bfloat16 [2048], P('tp'), may hold values from 0.099609375 to 1.8984375
Outputs:
- result: bfloat16 [1024, 2048], P(('grp', 'ep'), 'tp'), parts along dimension 0
There are 2 independent parts, one for each index of `grp`. A program takes and returns all parts, laid end to end along the dimension named above; an argument that names none is the same for every part. Nothing has to cross between parts.
Inputs may be any that keep to these rules, and one draw needn't show every extreme that they name: `routes`: each row names 4 different experts. Among the 64 rows of one index of ep at most 64 name the same expert, and in every draw some expert is named by exactly 64 rows of some index.
All inputs are finite; a program needn't handle non-finite values.
Results may differ from a plain program's by a relative error of at most 0.0077.
Values may be sent and summed in bfloat16 or wider, within the bound.
A program may use at most 64 MiB of HBM per device.

v0:
```python
import jax
import jax.numpy as jnp
from jax import lax
from jax.sharding import PartitionSpec as P

EPS = 1e-06


def swiglu_part(rows, gate_w, up_w, down_w):
    gate_value = jnp.dot(rows, gate_w, preferred_element_type=jnp.float32)
    up_value = jnp.dot(rows, up_w, preferred_element_type=jnp.float32)
    activated = (jax.nn.silu(gate_value) * up_value).astype(jnp.bfloat16)
    return jnp.dot(activated, down_w, preferred_element_type=jnp.float32)


def per_device(
    tokens,
    norm_gain,
    routes,
    route_weights,
    gate_experts,
    up_experts,
    down_experts,
    shared_gate,
    shared_up,
    shared_down,
    out_gain,
):
    tok_rows, model_width = tokens.shape
    per_token = routes.shape[1]
    experts = lax.axis_size("ep")
    tp_size = lax.axis_size("tp")
    half_width = model_width // tp_size
    capacity = 2 * tok_rows * per_token // experts
    wide_tokens = tokens.astype(jnp.float32)
    normed = (
        wide_tokens
        * lax.rsqrt(jnp.mean(wide_tokens * wide_tokens, axis=1, keepdims=True) + EPS)
        * norm_gain.astype(jnp.float32)
    ).astype(jnp.bfloat16)
    flat_routes = routes.reshape(-1)
    onehot = (flat_routes[:, None] == jnp.arange(experts, dtype=jnp.int32)[None, :]).astype(
        jnp.int32
    )
    before = jnp.cumsum(onehot, axis=0) - onehot
    slot_rank = jnp.sum(before * onehot, axis=1)
    slot_index = flat_routes * capacity + slot_rank
    source = jnp.arange(flat_routes.shape[0], dtype=jnp.int32) // per_token
    col_start = lax.axis_index("tp") * half_width
    outgoing = lax.dynamic_slice_in_dim(normed, col_start, half_width, 1)
    buffer = (
        jnp.zeros((experts * capacity, outgoing.shape[1]), jnp.bfloat16)
        .at[slot_index]
        .set(outgoing[source])
    )
    buffer = buffer.reshape(experts, capacity, outgoing.shape[1])
    received = lax.all_to_all(buffer, "ep", split_axis=0, concat_axis=0, tiled=True)
    received = lax.all_gather(received, "tp", axis=2, tiled=True)
    slot_count = received.shape[1]
    flat_rows = received.reshape(experts * slot_count, model_width)
    partial_value = swiglu_part(flat_rows, gate_experts[0], up_experts[0], down_experts[0])
    summed = lax.psum_scatter(
        partial_value.astype(jnp.bfloat16), "tp", scatter_dimension=1, tiled=True
    )
    returned = lax.all_to_all(
        summed.reshape(experts, slot_count, half_width),
        "ep",
        split_axis=0,
        concat_axis=0,
        tiled=True,
    )
    picked = returned.reshape(experts * capacity, half_width)[slot_index].astype(jnp.float32)
    weighted = picked * route_weights.reshape(-1)[:, None]
    routed = jnp.sum(weighted.reshape(tok_rows, per_token, half_width), axis=1)
    shared_partial = swiglu_part(normed, shared_gate, shared_up, shared_down)
    shared = lax.psum_scatter(
        shared_partial.astype(jnp.bfloat16), "tp", scatter_dimension=1, tiled=True
    ).astype(jnp.float32)
    mixed = shared + routed
    squares = lax.psum(jnp.sum(mixed * mixed, axis=1), "tp")
    inverse = lax.rsqrt(squares / model_width + EPS)
    return (mixed * inverse[:, None] * out_gain.astype(jnp.float32)[None, :]).astype(jnp.bfloat16)


def solution(mesh):
    in_specs = (
        P(("grp", "ep"), None),
        P(),
        P(("grp", "ep"), None),
        P(("grp", "ep"), None),
        P("ep", None, "tp"),
        P("ep", None, "tp"),
        P("ep", "tp", None),
        P(None, "tp"),
        P(None, "tp"),
        P("tp", None),
        P("tp"),
    )
    out_specs = P(("grp", "ep"), "tp")
    return jax.shard_map(
        per_device, mesh=mesh, in_specs=in_specs, out_specs=out_specs, check_vma=False
    )
```

profile of v0, /device:TPU:0, one launch (start us, length us, event | category | flops | bytes accessed | tf_op | source)
XLA Modules:
  0.0 124.3 jit_solution(17509838940911035079)
XLA Ops:
  6.5 0.0 copy-start
  6.5 0.0 all-gather.2.cloned.1.call-start
  6.5 0.8 broadcast_multiply_fusion
  7.3 0.8 copy.14
  8.1 0.1 eq.29
  8.2 0.1 eq.25
  8.3 1.1 fusion.7
  9.4 0.7 convert_element_type.45
  10.1 0.1 copy.13
  10.2 0.1 mul.88
  10.4 0.6 reduce-window.6
  10.9 0.2 slice_reduce_fusion
  11.2 0.1 fusion.26
  11.3 1.1 fusion.9
  12.4 3.7 %scatter_custom_fusion = bf16[512,1024]{1,0:T(8,128)(2,1)S(1)} fusion(s32[256]{0:T(256)S(1)} %bitcast.36, bf16[64,1024]{1,0:T(8,128)(2,1)S(1)} %constant_dynamic-slice_fusion, s32[1024]{0:T(1024)S(1)} %pad_clamp_fusion.1, bf16[]{:T(256)} %constant.42.clone.1), kind=kCustom, calls=%fused_computation.19 | custom fusion | bytes 1048578 | tf_op jit(solution)/shard_map/scatter | solution.py:54
  16.1 33.0 %all_to_all.10 = bf16[8,64,1024]{2,1,0:T(8,128)(2,1)} all-to-all(bf16[8,64,1024]{2,1,0:T(8,128)(2,1)S(1)} %bitcast.34), channel_id=1, replica_groups=mesh['grp'=2,'ep'=8,'tp'=2] {'ep'}, dimensions={0} | all-to-all | bytes 2097152 | tf_op jit(solution)/shard_map/all_to_all | solution.py:57
  49.1 0.0 all-gather.2.cloned.1.call-update
  49.1 0.0 reduce-scatter.5.cloned.1.call-start
  49.2 9.7 %all-gather.2.cloned.1.call-done = bf16[8,64,2048]{2,1,0:T(8,128)(2,1)} async-done(((bf16[8,64,1024]{2,1,0:T(8,128)(2,1)}), bf16[8,64,2048]{2,1,0:T(8,128)(2,1)}) %all-gather.2.cloned.1.call-update) | async-done | bytes 2097168 | tf_op jit(solution)/shard_map/all_gather | solution.py:58
  58.9 0.0 copy-start.4
  58.9 3.5 %fusion.5 = f32[512,256]{1,0:T(8,128)} fusion(bf16[512,2048]{1,0:T(8,128)(2,1)} %bitcast.40, bf16[1,2048,256]{2,1,0:T(8,128)(2,1)} %param.15), kind=kOutput, calls=%fused_computation.11 | convolution fusion | flops 536870912 | bytes 3670016 | tf_op jit(solution)/shard_map/dot_general | solution.py:10
  62.4 0.0 copy-done
  62.4 0.0 copy-done.4
  62.4 5.0 %convolution_convert_fusion = bf16[512,2048]{1,0:T(8,128)(2,1)} fusion(bf16[512,2048]{1,0:T(8,128)(2,1)S(1)} %bitcast.41, bf16[1,256,2048]{2,1,0:T(8,128)(2,1)S(1)} %copy-done, bf16[1,2048,256]{2,1,0:T(8,128)(2,1)} %param.16, f32[512,256]{1,0:T(8,128)} %fusion.5), kind=kOutput, calls=%fused_computation.3 | convolution fusion | flops 1075576832 | bytes 6815744 | tf_op jit(solution)/shard_map/dot_general | solution.py:13
  67.4 0.0 copy-start.1
  67.4 0.0 reduce-scatter.5.cloned.1.call-update
  67.4 11.0 %reduce-scatter.5.cloned.1.call-done = bf16[512,1024]{1,0:T(8,128)(2,1)} async-done(((bf16[512,2048]{1,0:T(8,128)(2,1)}), bf16[512,1024]{1,0:T(8,128)(2,1)}) %reduce-scatter.5.cloned.1.call-update) | async-done | bytes 1048592 | tf_op jit(solution)/shard_map/reduce_scatter | solution.py:62
  78.4 5.9 %all-to-all-start.1 = ((bf16[8,64,1024]{2,1,0:T(8,128)(2,1)}), bf16[8,64,1024]{2,1,0:T(8,128)(2,1)S(1)}, u32[]{:S(2)}, u32[]{:S(2)}) async-start(bf16[8,64,1024]{2,1,0:T(8,128)(2,1)} %bitcast.35), calls=%async_computation.3 | async-start | bytes 2097152 | tf_op jit(solution)/shard_map/all_to_all | solution.py:65
  84.3 0.0 copy-start.2
  84.3 0.0 copy-start.3
  84.3 0.0 reduce-scatter.3.cloned.1.call-start
  84.3 0.0 copy-done.1
  84.4 0.3 fusion.30
  84.7 3.0 %convolution_convert_fusion.1 = bf16[64,2048]{1,0:T(8,128)(2,1)} fusion(bf16[256,2048]{1,0:T(8,128)(2,1)} %param.20, bf16[64,2048]{1,0:T(8,128)(2,1)S(1)} %fusion.9, bf16[2048,256]{1,0:T(8,128)(2,1)} %param.19, f32[64,256]{1,0:T(8,128)S(1)} %fusion.30), kind=kOutput, calls=%fused_computation.4 | convolution fusion | flops 134447104 | bytes 2686976 | tf_op jit(solution)/shard_map/dot_general | solution.py:13
  87.7 0.0 reduce-scatter.3.cloned.1.call-update
  87.7 0.0 copy-done.2
  87.7 0.0 copy-done.3
  87.7 0.1 copy.16
  87.9 22.5 %all-to-all-done.1 = bf16[8,64,1024]{2,1,0:T(8,128)(2,1)S(1)} async-done(((bf16[8,64,1024]{2,1,0:T(8,128)(2,1)}), bf16[8,64,1024]{2,1,0:T(8,128)(2,1)S(1)}, u32[]{:S(2)}, u32[]{:S(2)}) %all-to-all-start.1) | async-done | bytes 1048608 | tf_op jit(solution)/shard_map/all_to_all | solution.py:65
  110.4 1.2 gather_fusion
  111.5 0.3 reshape.127
  111.9 0.7 multiply_reduce_fusion
  112.6 0.0 reduce-scatter.3.cloned.1.call-done
  112.6 1.0 multiply_reduce_fusion.1
  113.7 2.5 %psum.7 = f32[64]{0:T(128)S(1)} all-reduce(f32[64]{0:T(128)S(1)} %multiply_reduce_fusion.1), channel_id=1, replica_groups=mesh['grp'=2,'ep'=8,'tp'=2] {'tp'}, use_global_device_ids=true, to_apply=%region_9.10 | all-reduce | flops 64 | bytes 512 | tf_op jit(solution)/shard_map/psum | solution.py:80
  116.1 1.7 %multiply_convert_fusion = bf16[64,1024]{1,0:T(8,128)(2,1)} fusion(f32[64,1024]{1,0:T(8,128)S(1)} %multiply_reduce_fusion, bf16[64,1024]{1,0:T(8,128)(2,1)} %reduce-scatter.3.cloned.1.call-done, f32[1024]{0:T(1024)S(1)} %convert_element_type.56, f32[64]{0:T(128)S(1)} %add_rsqrt_fusion), kind=kLoop, calls=%fused_computation.27 | loop fusion | flops 327680 | bytes 528640 | tf_op jit(solution)/shard_map/convert_element_type | solution.py:82
  (11 shorter events, 0.1 us)
Async XLA Ops:
  6.5 55.9 %copy-start = (bf16[1,256,2048]{2,1,0:T(8,128)(2,1)S(1)}, bf16[1,256,2048]{2,1,0:T(8,128)(2,1)}, u32[]{:S(2)}) copy-start(bf16[1,256,2048]{2,1,0:T(8,128)(2,1)} %param.17) | copy-start | bytes 3145732
  6.5 52.3 %all-gather.2.cloned.1.call-start = ((), (), s32[]{:S(2)}) async-start(), calls=%async_computation.5 | async-start | bytes 3145728 | tf_op jit(solution)/shard_map/all_gather | solution.py:58
  49.1 29.3 %reduce-scatter.5.cloned.1.call-start = ((), (), s32[]{:S(2)}) async-start(), calls=%async_computation.6 | async-start | bytes 3145728 | tf_op jit(solution)/shard_map/reduce_scatter | solution.py:62
  58.9 3.5 %copy-start.4 = (bf16[8,64,2048]{2,1,0:T(8,128)(2,1)S(1)}, bf16[8,64,2048]{2,1,0:T(8,128)(2,1)}, u32[]{:S(2)}) copy-start(bf16[8,64,2048]{2,1,0:T(8,128)(2,1)} %all-gather.2.cloned.1.call-done) | copy-start | bytes 6291460
  67.4 16.9 %copy-start.1 = (bf16[2048,256]{1,0:T(8,128)(2,1)S(1)}, bf16[2048,256]{1,0:T(8,128)(2,1)}, u32[]{:S(2)}) copy-start(bf16[2048,256]{1,0:T(8,128)(2,1)} %param.18) | copy-start | bytes 3145732
  78.4 32.0 %all-to-all-start.1 = ((bf16[8,64,1024]{2,1,0:T(8,128)(2,1)}), bf16[8,64,1024]{2,1,0:T(8,128)(2,1)S(1)}, u32[]{:S(2)}, u32[]{:S(2)}) async-start(bf16[8,64,1024]{2,1,0:T(8,128)(2,1)} %bitcast.35), calls=%async_computation.3 | async-start | bytes 2097152 | tf_op jit(solution)/shard_map/all_to_all | solution.py:65
  84.3 3.4 %copy-start.2 = (bf16[1024]{0:T(1024)(128)(2,1)S(1)}, bf16[1024]{0:T(1024)(128)(2,1)}, u32[]{:S(2)}) copy-start(bf16[1024]{0:T(1024)(128)(2,1)} %param.21) | copy-start | bytes 6148
  84.3 3.5 %copy-start.3 = (f32[64,4]{0,1:T(4,128)S(1)}, f32[64,4]{0,1:T(4,128)}, u32[]{:S(2)}) copy-start(f32[64,4]{0,1:T(4,128)} %param.14) | copy-start | bytes 3076
  84.3 28.3 %reduce-scatter.3.cloned.1.call-start = ((), (), s32[]{:S(2)}) async-start(), calls=%async_computation.4 | async-start | bytes 393216 | tf_op jit(solution)/shard_map/reduce_scatter | solution.py:76
Sparse Core Ops, SparseCore 0:
  49.2 9.5 all-gather.1
  67.6 10.7 reduce-scatter.4
  87.8 9.1 reduce-scatter.2
where the time goes:
time: 125 us; the launch traced here: 124 us
  waiting for transfers between devices  43.2 us (35%)
  blocking collectives  35.4 us (28%)
  between operations  13.3 us (11%)
  matrix products  11.9 us (10%)
  other arithmetic  7.82 us (6%)
  local copies, waits for them, and re-layouts  6.73 us (5%)
  starting transfers between devices  5.98 us (5%)
    all_to_all x1, blocking collectives, per_device(): lax.all_to_all(buffer, 'ep', split_axis=0, concat_axis=0, tiled=True)  33 us
    all_to_all x1, waiting for transfers between devices, per_device(): lax.all_to_all(summed.reshape(experts, slot_count, half_width), 'ep', spl...  22.5 us
    reduce_scatter x1, waiting for transfers between devices, per_device(): lax.psum_scatter(partial_value.astype(jnp.bfloat16), 'tp', scatter_dimens...  11 us
    all_gather x1, waiting for transfers between devices, per_device(): received = lax.all_gather(received, 'tp', axis=2, tiled=True)  9.69 us
    dot_general x2, matrix products, swiglu_part(): return jnp.dot(activated, down_w, preferred_element_type=jnp.float32)  8.06 us
    all_to_all x1, starting transfers between devices, per_device(): lax.all_to_all(summed.reshape(experts, slot_count, half_width), 'ep', spl...  5.9 us
    dot_general x2, matrix products, swiglu_part(): gate_value = jnp.dot(rows, gate_w, preferred_element_type=jnp.float32)  3.81 us
    scatter x1, local copies, waits for them, and re-layouts, per_device(): buffer = jnp.zeros((experts * capacity, outgoing.shape[1]), jnp.bfloat16)...  3.71 us
  transfers between devices with their start and end apart: 4, of which 3 were waited for; matrix products, arithmetic and copies ran while one was open for 5% of the time, Pallas kernels for 0%

commit v1 on v0

v1 whole, which is shorter than its diff:
```python
import functools

import jax
import jax.numpy as jnp
from jax import lax
from jax.experimental import pallas as pl
from jax.experimental.pallas import tpu as pltpu
from jax.sharding import PartitionSpec as P

EPS = 1e-06
MESH = pl.DeviceIdType.MESH
LANES = 128
HALF_LANES = LANES // 2


def xor(a, b, size):
    total, bit = 0, 1
    while bit < size:
        total = total + ((a // bit + b // bit) % 2) * bit
        bit *= 2
    return total


def kernel(
    ep,
    tokens_ref,
    norm_gain_ref,
    routes_ref,
    weights_ref,
    gate_hbm,
    up_hbm,
    down_hbm,
    sgate_hbm,
    sup_hbm,
    sdown_hbm,
    out_gain_ref,
    result_ref,
    gathered,
    gate,
    up,
    down,
    sgate,
    sup,
    sdown,
    kept,
    shared_kept,
    core_out,
    core_in,
    score_out,
    score_in,
    y_out,
    y_in,
    z_out,
    z_in,
    local_sum,
    sq_out,
    sq_in,
    load_sem,
    z_send,
    z_recv,
    y_send,
    y_recv,
    cz_send,
    cz_recv,
    cy_send,
    cy_recv,
    co_send,
    co_recv,
    yo_send,
    yo_recv,
    zo_send,
    zo_recv,
    sq_send,
    sq_recv,
):
    zs = ep // 2
    rows, width = tokens_ref.shape
    half_rows, half_width = rows // 2, width // 2
    me = lax.axis_index("ep")
    core = lax.axis_index("tp")
    z, y = me // 2, me % 2
    zz = [xor(z, s, zs) for s in range(zs)]
    sibling = {"tp": 1 - core}
    across = {"ep": z * 2 + (1 - y)}
    along = [{"ep": zz[s] * 2 + y} for s in range(zs)]

    loads = []
    for i, (src, dst) in enumerate(
        [
            (sgate_hbm, sgate),
            (sup_hbm, sup),
            (sdown_hbm, sdown),
            (gate_hbm.at[0], gate),
            (up_hbm.at[0], up),
            (down_hbm.at[0], down),
        ]
    ):
        copy = pltpu.make_async_copy(src, dst, load_sem.at[i])
        copy.start()
        loads.append(copy)

    barrier = pltpu.get_barrier_semaphore()
    peers = [sibling, across] + along[1:]
    for peer in peers:
        pl.semaphore_signal(barrier, inc=1, device_id=peer, device_id_type=MESH)

    wide = tokens_ref[...].astype(jnp.float32)
    scale = lax.rsqrt(jnp.mean(wide * wide, axis=1, keepdims=True) + EPS)
    gain = norm_gain_ref[...].astype(jnp.float32)
    gathered[me, :, :width] = (wide * scale * gain).astype(jnp.bfloat16)
    lane = lax.broadcasted_iota(jnp.int32, (rows, LANES), 1)
    chosen = jnp.zeros((rows, LANES), jnp.float32)
    for k in range(routes_ref.shape[1]):
        hit = routes_ref[:, k : k + 1] == lane % HALF_LANES
        chosen = chosen + jnp.where(hit, weights_ref[:, k : k + 1], 0.0)
    high = chosen.astype(jnp.bfloat16).astype(jnp.float32)
    gathered[me, :, width:] = jnp.where(lane < HALF_LANES, high, chosen - high).astype(
        jnp.bfloat16
    )

    pl.semaphore_wait(barrier, len(peers))

    my_rows = pl.ds(pl.multiple_of(core * half_rows, half_rows), half_rows)
    other_rows = pl.ds(pl.multiple_of((1 - core) * half_rows, half_rows), half_rows)
    my_cols = pl.ds(pl.multiple_of(core * half_width, half_width), half_width)
    other_cols = pl.ds(pl.multiple_of((1 - core) * half_width, half_width), half_width)

    sent = []

    def send(src, dst, send_sem, recv_sem, target):
        copy = pltpu.make_async_remote_copy(
            src_ref=src,
            dst_ref=dst,
            send_sem=send_sem,
            recv_sem=recv_sem,
            device_id=target,
            device_id_type=MESH,
        )
        copy.start()
        sent.append(copy)
        return copy

    def arrived(ref, send_sem, recv_sem, target):
        pltpu.make_async_remote_copy(
            src_ref=ref,
            dst_ref=ref,
            send_sem=send_sem,
            recv_sem=recv_sem,
            device_id=target,
            device_id_type=MESH,
        ).wait_recv()

    own = gathered.at[me, my_rows]
    send(own, own, y_send.at[0], y_recv.at[0], across)
    for s in range(1, zs):
        send(own, own, z_send.at[s], z_recv.at[s], along[s])

    def take_z(s):
        block = gathered.at[zz[s] * 2 + y, my_rows]
        arrived(block, z_send.at[s], z_recv.at[s], along[s])
        send(block, block, y_send.at[s], y_recv.at[s], across)
        send(block, block, cz_send.at[s], cz_recv.at[s], sibling)

    def take_y(s):
        block = gathered.at[zz[s] * 2 + (1 - y), my_rows]
        arrived(block, y_send.at[s], y_recv.at[s], across)
        send(block, block, cy_send.at[s], cy_recv.at[s], sibling)

    def take_core(s):
        if s > 0:
            block = gathered.at[zz[s] * 2 + y, other_rows]
            arrived(block, cz_send.at[s], cz_recv.at[s], sibling)
        block = gathered.at[zz[s] * 2 + (1 - y), other_rows]
        arrived(block, cy_send.at[s], cy_recv.at[s], sibling)

    def swiglu(x, gate_w, up_w):
        g = jnp.dot(x, gate_w[...], preferred_element_type=jnp.float32)
        u = jnp.dot(x, up_w[...], preferred_element_type=jnp.float32)
        return (g / (1.0 + jnp.exp(-g)) * u).astype(jnp.bfloat16)

    def experts(s):
        pair = gathered.at[pl.ds(zz[s] * 2, 2)]
        x = pair[:, :, :width].reshape(2 * rows, width)
        act = swiglu(x, gate, up)
        core_out[s] = jnp.dot(
            act, down[:, other_cols], preferred_element_type=jnp.float32
        ).astype(jnp.bfloat16)
        send(core_out.at[s], core_in.at[s], co_send.at[s], co_recv.at[s], sibling)
        kept[s] = jnp.dot(act, down[:, my_cols], preferred_element_type=jnp.float32)

    def weight_of(block):
        spread = gathered[block, :, width:].astype(jnp.float32)
        return jnp.sum(
            jnp.where(lane % HALF_LANES == me, spread, 0.0), axis=1, keepdims=True
        )

    def combine(s):
        arrived(core_in.at[s], co_send.at[s], co_recv.at[s], sibling)
        theirs = pl.ds(pl.multiple_of((1 - y) * rows, rows), rows)
        value = kept[s, theirs] + core_in[s, theirs].astype(jnp.float32)
        y_out[s] = (value * weight_of(zz[s] * 2 + (1 - y))).astype(jnp.bfloat16)
        send(y_out.at[s], y_in.at[s], yo_send.at[s], yo_recv.at[s], across)

    def finish(s):
        mine = pl.ds(pl.multiple_of(y * rows, rows), rows)
        value = kept[s, mine] + core_in[s, mine].astype(jnp.float32)
        value = value * weight_of(zz[s] * 2 + y)
        arrived(y_in.at[s], yo_send.at[s], yo_recv.at[s], across)
        value = value + y_in[s].astype(jnp.float32)
        if s == 0:
            local_sum[...] = value
        else:
            z_out[s] = value.astype(jnp.bfloat16)
            send(z_out.at[s], z_in.at[s], zo_send.at[s], zo_recv.at[s], along[s])

    for i in range(3):
        loads[i].wait()
    act = swiglu(gathered[me, :, :width], sgate, sup)
    score_out[...] = jnp.dot(
        act, sdown[:, other_cols], preferred_element_type=jnp.float32
    ).astype(jnp.bfloat16)
    send(score_out, score_in, co_send.at[zs], co_recv.at[zs], sibling)
    shared_kept[...] = jnp.dot(act, sdown[:, my_cols], preferred_element_type=jnp.float32)
    for i in range(3, 6):
        loads[i].wait()

    for s in range(zs + 2):
        if s < zs:
            if s + 1 < zs:
                if s == 0:
                    take_y(0)
                take_z(s + 1)
            if s > 0 or zs == 1:
                take_y(s)
            take_core(s)
            experts(s)
        if 1 <= s <= zs:
            combine(s - 1)
        if s >= 2:
            finish(s - 2)

    arrived(score_in, co_send.at[zs], co_recv.at[zs], sibling)
    mixed = local_sum[...] + (shared_kept[...] + score_in[...].astype(jnp.float32))
    for s in range(1, zs):
        arrived(z_in.at[s], zo_send.at[s], zo_recv.at[s], along[s])
        mixed = mixed + z_in[s].astype(jnp.float32)
    local_sum[...] = mixed
    squares = jnp.sum(mixed * mixed, axis=1, keepdims=True)
    sq_out[...] = jnp.broadcast_to(squares, sq_out.shape)
    send(sq_out, sq_in, sq_send, sq_recv, sibling)
    arrived(sq_in, sq_send, sq_recv, sibling)
    inverse = lax.rsqrt((squares + sq_in[:, :1]) / width + EPS)
    result_ref[...] = (
        local_sum[...] * inverse * out_gain_ref[...].astype(jnp.float32)
    ).astype(jnp.bfloat16)
    for copy in sent:
        copy.wait_send()


def per_device(tokens, norm_gain, routes, route_weights, gate, up, down, sgate, sup, sdown, out_gain):
    ep = lax.axis_size("ep")
    zs = ep // 2
    rows, width = tokens.shape
    hidden, shidden = gate.shape[2], sgate.shape[1]
    half = width // 2
    bf, f32 = jnp.bfloat16, jnp.float32
    vmem = pl.BlockSpec(memory_space=pltpu.VMEM)
    hbm = pl.BlockSpec(memory_space=pl.ANY)
    dma = pltpu.SemaphoreType.DMA
    flops = 6 * rows * width * (ep * hidden + shidden)
    return pl.pallas_call(
        functools.partial(kernel, ep),
        out_shape=jax.ShapeDtypeStruct((rows, half), bf),
        in_specs=[vmem] * 4 + [hbm] * 6 + [vmem],
        out_specs=vmem,
        scratch_shapes=[
            pltpu.VMEM((ep, rows, width + LANES), bf),
            pltpu.VMEM((width, hidden), bf),
            pltpu.VMEM((width, hidden), bf),
            pltpu.VMEM((hidden, width), bf),
            pltpu.VMEM((width, shidden), bf),
            pltpu.VMEM((width, shidden), bf),
            pltpu.VMEM((shidden, width), bf),
            pltpu.VMEM((zs, 2 * rows, half), f32),
            pltpu.VMEM((rows, half), f32),
            pltpu.VMEM((zs, 2 * rows, half), bf),
            pltpu.VMEM((zs, 2 * rows, half), bf),
            pltpu.VMEM((rows, half), bf),
            pltpu.VMEM((rows, half), bf),
            pltpu.VMEM((zs, rows, half), bf),
            pltpu.VMEM((zs, rows, half), bf),
            pltpu.VMEM((zs, rows, half), bf),
            pltpu.VMEM((zs, rows, half), bf),
            pltpu.VMEM((rows, half), f32),
            pltpu.VMEM((rows, LANES), f32),
            pltpu.VMEM((rows, LANES), f32),
            dma((6,)),
            dma((zs,)),
            dma((zs,)),
            dma((zs,)),
            dma((zs,)),
            dma((zs,)),
            dma((zs,)),
            dma((zs,)),
            dma((zs,)),
            dma((zs + 1,)),
            dma((zs + 1,)),
            dma((zs,)),
            dma((zs,)),
            dma((zs,)),
            dma((zs,)),
            dma,
            dma,
        ],
        compiler_params=pltpu.CompilerParams(
            collective_id=0, has_side_effects=True, vmem_limit_bytes=60 * 1024 * 1024
        ),
        cost_estimate=pl.CostEstimate(
            flops=flops, bytes_accessed=6 * width * (hidden + shidden), transcendentals=0
        ),
    )(
        tokens,
        norm_gain.reshape(1, -1),
        routes,
        route_weights,
        gate,
        up,
        down,
        sgate,
        sup,
        sdown,
        out_gain.reshape(1, -1),
    )


def solution(mesh):
    in_specs = (
        P(("grp", "ep"), None),
        P(),
        P(("grp", "ep"), None),
        P(("grp", "ep"), None),
        P("ep", None, "tp"),
        P("ep", None, "tp"),
        P("ep", "tp", None),
        P(None, "tp"),
        P(None, "tp"),
        P("tp", None),
        P("tp"),
    )
    out_specs = P(("grp", "ep"), "tp")
    return jax.shard_map(
        per_device, mesh=mesh, in_specs=in_specs, out_specs=out_specs, check_vma=False
    )
```

time: 125 us -> 51.2 us (0.41)
  Pallas kernels: 0 us -> 46 us
  waiting for transfers between devices: 43.2 us -> 0 us
  blocking collectives: 35.4 us -> 0 us
  between operations: 13.3 us -> 0.01 us
  matrix products: 11.9 us -> 0 us
  other arithmetic: 7.82 us -> 0 us
  starting transfers between devices: 5.98 us -> 0 us
  local copies, waits for them, and re-layouts: 6.73 us -> 4.97 us
    pallas_call x0 -> x1, Pallas kernels: none -> 46 us  [per_device(): pl.pallas_call(functools.partial(kernel, ep), out_shape=jax.ShapeDtypeStr...]
    all_to_all x1 -> x0, blocking collectives: 33 us -> none  [per_device(): lax.all_to_all(buffer, 'ep', split_axis=0, concat_axis=0, tiled=True)]
    all_to_all x1 -> x0, waiting for transfers between devices: 22.5 us -> none  [per_device(): lax.all_to_all(summed.reshape(experts, slot_count, half_width), 'ep', spl...]
    dot_general x4 -> x0, matrix products: 11.9 us -> none  [the longest x2 8.06 us: swiglu_part(): return jnp.dot(activated, down_w, preferred_element_type=jnp.float32)]
    reduce_scatter x2 -> x0, waiting for transfers between devices: 11 us -> none  [the longest x1 11 us: per_device(): lax.psum_scatter(partial_value.astype(jnp.bfloat16), 'tp', scatter_dimens...]
    all_gather x1 -> x0, waiting for transfers between devices: 9.69 us -> none  [per_device(): received = lax.all_gather(received, 'tp', axis=2, tiled=True)]
    all_to_all x1 -> x0, starting transfers between devices: 5.9 us -> none  [per_device(): lax.all_to_all(summed.reshape(experts, slot_count, half_width), 'ep', spl...]
    scatter x1 -> x0, local copies, waits for them, and re-layouts: 3.71 us -> none  [per_device(): buffer = jnp.zeros((experts * capacity, outgoing.shape[1]), jnp.bfloat16)...]
  transfers between devices with their start and end apart: 4 -> 0, of which waited for: 3 -> 0; matrix products, arithmetic and copies ran while one was open for 5% -> 0% of each run, Pallas kernels for 0% -> 0%
where the time goes in v1:
time: 51.2 us; the launch traced here: 51 us
  Pallas kernels  46 us (90%)
  local copies, waits for them, and re-layouts  4.97 us (10%)
    pallas_call x1, Pallas kernels, per_device(): pl.pallas_call(functools.partial(kernel, ep), out_shape=jax.ShapeDtypeStr...  46 us
    unnamed x9, local copies, waits for them, and re-layouts  3.08 us
    reshape x1, local copies, waits for them, and re-layouts, per_device(): out_gain.reshape(1, -1)  1.28 us

profile of v1, /device:TPU:0, one launch (start us, length us, event | category | flops | bytes accessed | tf_op | source)
XLA Modules:
  0.0 51.0 jit_solution(675757642173039857)
XLA Ops:
  0.0 0.0 copy-start
  0.0 1.3 %reshape.7.out_gain_ref = bf16[1,1024]{1,0:T(2,128)(2,1)} reshape(bf16[1024]{0:T(1024)(128)(2,1)} %param.21) | data formatting | bytes 4096 | tf_op jit(solution)/shard_map/reshape | solution.py:332
  1.3 0.0 copy-done
  1.3 0.0 copy-start.1
  1.3 0.6 %reshape.6.norm_gain_ref = bf16[1,2048]{1,0:T(2,128)(2,1)} reshape(bf16[2048]{0:T(1024)(128)(2,1)S(1)} %copy-done) | data formatting | bytes 8192 | tf_op jit(solution)/shard_map/reshape | solution.py:323
  1.9 0.1 copy-done.1
  2.0 0.0 copy-start.2
  2.0 0.7 %copy.12.routes_ref = s32[64,4]{1,0:T(8,128)} copy(s32[64,4]{0,1:T(4,128)S(1)} %copy-done.1) | data formatting | bytes 2048 | tf_op args[2]
  2.7 0.0 copy-done.2
  2.7 0.7 %copy.13.weights_ref = f32[64,4]{1,0:T(8,128)} copy(f32[64,4]{0,1:T(4,128)S(1)} %copy-done.2) | data formatting | bytes 2048 | tf_op args[3]
  3.4 46.0 %shard_map.109 = bf16[64,1024]{1,0:T(8,128)(2,1)} custom-call(bf16[64,2048]{1,0:T(8,128)(2,1)} %tokens_ref.1, bf16[1,2048]{1,0:T(2,128)(2,1)} %reshape.6.norm_gain_ref, s32[64,4]{1,0:T(8,128)} %copy.12.routes_ref, f32[64,4]{1,0:T(8,128)} %copy.13.weights_ref, bf16[1,2048,256]{2,1,0:T(8,128)(2,1)} %gate_hbm.1, bf16[1,2048,256]{2,1,0:T(8,128)(2,1)} %up_hbm.1, ...), custom_call_target="tpu_custom_call" | custom-call | flops 1811939328 | bytes 6291456 | tf_op jit(solution)/shard_map/pallas_call | solution.py:271
  49.5 1.6 %copy.15 = bf16[64,1024]{1,0:T(8,128)(2,1)} copy(bf16[64,1024]{1,0:T(8,128)(2,1)} %shard_map.109) | data formatting | bytes 262144
Async XLA Ops:
  0.0 1.3 %copy-start = (bf16[2048]{0:T(1024)(128)(2,1)S(1)}, bf16[2048]{0:T(1024)(128)(2,1)}, u32[]{:S(2)}) copy-start(bf16[2048]{0:T(1024)(128)(2,1)} %param.12) | copy-start | bytes 12292
  1.3 0.7 %copy-start.1 = (s32[64,4]{0,1:T(4,128)S(1)}, s32[64,4]{0,1:T(4,128)}, u32[]{:S(2)}) copy-start(s32[64,4]{0,1:T(4,128)} %param.13) | copy-start | bytes 3076
  2.0 0.7 %copy-start.2 = (f32[64,4]{0,1:T(4,128)S(1)}, f32[64,4]{0,1:T(4,128)}, u32[]{:S(2)}) copy-start(f32[64,4]{0,1:T(4,128)} %param.14) | copy-start | bytes 3076

commit v2 on v1

--- a/solution.py
+++ b/solution.py
@@ -13,12 +13,18 @@
 HALF_LANES = LANES // 2
 
 
-def xor(a, b, size):
-    total, bit = 0, 1
-    while bit < size:
-        total = total + ((a // bit + b // bit) % 2) * bit
-        bit *= 2
-    return total
+PIECES = 2
+
+
+def by_distance(z, zs):
+    table = [sorted(range(zs), key=lambda o: (abs(o - at), -o)) for at in range(zs)]
+    order = []
+    for k in range(zs):
+        pick = table[0][k]
+        for at in range(1, zs):
+            pick = jnp.where(z == at, table[at][k], pick)
+        order.append(pick)
+    return order
 
 
 def kernel(
@@ -56,7 +62,8 @@
     sq_out,
     sq_in,
     load_sem,
-    z_send,
+    r_send,
+    l_send,
     z_recv,
     y_send,
     y_recv,
@@ -79,7 +86,7 @@
     me = lax.axis_index("ep")
     core = lax.axis_index("tp")
     z, y = me // 2, me % 2
-    zz = [xor(z, s, zs) for s in range(zs)]
+    zz = by_distance(z, zs)
     sibling = {"tp": 1 - core}
     across = {"ep": z * 2 + (1 - y)}
     along = [{"ep": zz[s] * 2 + y} for s in range(zs)]
@@ -87,12 +94,12 @@
     loads = []
     for i, (src, dst) in enumerate(
         [
+            (gate_hbm.at[0], gate),
+            (up_hbm.at[0], up),
+            (down_hbm.at[0], down),
             (sgate_hbm, sgate),
             (sup_hbm, sup),
             (sdown_hbm, sdown),
-            (gate_hbm.at[0], gate),
-            (up_hbm.at[0], up),
-            (down_hbm.at[0], down),
         ]
     ):
         copy = pltpu.make_async_copy(src, dst, load_sem.at[i])
@@ -106,13 +113,15 @@
 
     wide = tokens_ref[...].astype(jnp.float32)
     scale = lax.rsqrt(jnp.mean(wide * wide, axis=1, keepdims=True) + EPS)
-    gain = norm_gain_ref[...].astype(jnp.float32)
+    gain = norm_gain_ref[...].astype(jnp.float32).reshape(1, width)
     gathered[me, :, :width] = (wide * scale * gain).astype(jnp.bfloat16)
     lane = lax.broadcasted_iota(jnp.int32, (rows, LANES), 1)
-    chosen = jnp.zeros((rows, LANES), jnp.float32)
-    for k in range(routes_ref.shape[1]):
-        hit = routes_ref[:, k : k + 1] == lane % HALF_LANES
-        chosen = chosen + jnp.where(hit, weights_ref[:, k : k + 1], 0.0)
+    expert = lax.broadcasted_iota(jnp.int32, (LANES, rows), 0) % HALF_LANES
+    chosen = jnp.zeros((LANES, rows), jnp.float32)
+    for k in range(routes_ref.shape[0]):
+        hit = routes_ref[k : k + 1, :] == expert
+        chosen = chosen + jnp.where(hit, weights_ref[k : k + 1, :], 0.0)
+    chosen = chosen.T
     high = chosen.astype(jnp.bfloat16).astype(jnp.float32)
     gathered[me, :, width:] = jnp.where(lane < HALF_LANES, high, chosen - high).astype(
         jnp.bfloat16
@@ -120,8 +129,11 @@
 
     pl.semaphore_wait(barrier, len(peers))
 
-    my_rows = pl.ds(pl.multiple_of(core * half_rows, half_rows), half_rows)
-    other_rows = pl.ds(pl.multiple_of((1 - core) * half_rows, half_rows), half_rows)
+    piece = half_rows // PIECES
+
+    def rows_of(which, q):
+        return pl.ds(pl.multiple_of(which * half_rows + q * piece, piece), piece)
+
     my_cols = pl.ds(pl.multiple_of(core * half_width, half_width), half_width)
     other_cols = pl.ds(pl.multiple_of((1 - core) * half_width, half_width), half_width)
 
@@ -150,28 +162,48 @@
             device_id_type=MESH,
         ).wait_recv()
 
-    own = gathered.at[me, my_rows]
-    send(own, own, y_send.at[0], y_recv.at[0], across)
-    for s in range(1, zs):
-        send(own, own, z_send.at[s], z_recv.at[s], along[s])
+    passed = []
+
+    def pass_on(block, q, source, sends, target, when):
+        copy = pltpu.make_async_remote_copy(
+            src_ref=block,
+            dst_ref=block,
+            send_sem=sends.at[source, q],
+            recv_sem=z_recv.at[source, q],
+            device_id={"ep": target * 2 + y},
+            device_id_type=MESH,
+        )
+        pl.when(when)(copy.start)
+        passed.append((copy, when))
+
+    for q in range(PIECES):
+        own = gathered.at[me, rows_of(core, q)]
+        pass_on(own, q, z, r_send, z + 1, z < zs - 1)
+        pass_on(own, q, z, l_send, z - 1, z > 0)
+        send(own, own, y_send.at[0, q], y_recv.at[0, q], across)
 
     def take_z(s):
-        block = gathered.at[zz[s] * 2 + y, my_rows]
-        arrived(block, z_send.at[s], z_recv.at[s], along[s])
-        send(block, block, y_send.at[s], y_recv.at[s], across)
-        send(block, block, cz_send.at[s], cz_recv.at[s], sibling)
+        for q in range(PIECES):
+            block = gathered.at[zz[s] * 2 + y, rows_of(core, q)]
+            arrived(block, r_send.at[zz[s], q], z_recv.at[zz[s], q], across)
+            pass_on(block, q, zz[s], r_send, z + 1, jnp.logical_and(zz[s] < z, z < zs - 1))
+            pass_on(block, q, zz[s], l_send, z - 1, jnp.logical_and(zz[s] > z, z > 0))
+            send(block, block, y_send.at[s, q], y_recv.at[s, q], across)
+            send(block, block, cz_send.at[s, q], cz_recv.at[s, q], sibling)
 
     def take_y(s):
-        block = gathered.at[zz[s] * 2 + (1 - y), my_rows]
-        arrived(block, y_send.at[s], y_recv.at[s], across)
-        send(block, block, cy_send.at[s], cy_recv.at[s], sibling)
+        for q in range(PIECES):
+            block = gathered.at[zz[s] * 2 + (1 - y), rows_of(core, q)]
+            arrived(block, y_send.at[s, q], y_recv.at[s, q], across)
+            send(block, block, cy_send.at[s, q], cy_recv.at[s, q], sibling)
 
     def take_core(s):
-        if s > 0:
-            block = gathered.at[zz[s] * 2 + y, other_rows]
-            arrived(block, cz_send.at[s], cz_recv.at[s], sibling)
-        block = gathered.at[zz[s] * 2 + (1 - y), other_rows]
-        arrived(block, cy_send.at[s], cy_recv.at[s], sibling)
+        for q in range(PIECES):
+            if s > 0:
+                block = gathered.at[zz[s] * 2 + y, rows_of(1 - core, q)]
+                arrived(block, cz_send.at[s, q], cz_recv.at[s, q], sibling)
+            block = gathered.at[zz[s] * 2 + (1 - y), rows_of(1 - core, q)]
+            arrived(block, cy_send.at[s, q], cy_recv.at[s, q], sibling)
 
     def swiglu(x, gate_w, up_w):
         g = jnp.dot(x, gate_w[...], preferred_element_type=jnp.float32)
@@ -211,39 +243,48 @@
             local_sum[...] = value
         else:
             z_out[s] = value.astype(jnp.bfloat16)
-            send(z_out.at[s], z_in.at[s], zo_send.at[s], zo_recv.at[s], along[s])
-
-    for i in range(3):
-        loads[i].wait()
-    act = swiglu(gathered[me, :, :width], sgate, sup)
-    score_out[...] = jnp.dot(
-        act, sdown[:, other_cols], preferred_element_type=jnp.float32
-    ).astype(jnp.bfloat16)
-    send(score_out, score_in, co_send.at[zs], co_recv.at[zs], sibling)
-    shared_kept[...] = jnp.dot(act, sdown[:, my_cols], preferred_element_type=jnp.float32)
-    for i in range(3, 6):
-        loads[i].wait()
-
-    for s in range(zs + 2):
-        if s < zs:
-            if s + 1 < zs:
-                if s == 0:
-                    take_y(0)
-                take_z(s + 1)
-            if s > 0 or zs == 1:
-                take_y(s)
-            take_core(s)
-            experts(s)
-        if 1 <= s <= zs:
+            send(z_out.at[s], z_in.at[z], zo_send.at[s], zo_recv.at[z], along[s])
+
+    def shared_expert():
+        for i in range(3, 6):
+            loads[i].wait()
+        act = swiglu(gathered[me, :, :width], sgate, sup)
+        score_out[...] = jnp.dot(
+            act, sdown[:, other_cols], preferred_element_type=jnp.float32
+        ).astype(jnp.bfloat16)
+        send(score_out, score_in, co_send.at[zs], co_recv.at[zs], sibling)
+        shared_kept[...] = jnp.dot(act, sdown[:, my_cols], preferred_element_type=jnp.float32)
+
+    ahead = 2
+    for s in range(1, min(1 + ahead, zs)):
+        take_z(s)
+    for s in range(zs):
+        take_y(s)
+        take_core(s)
+        if s == 0:
+            for i in range(3):
+                loads[i].wait()
+        experts(s)
+        if s + 1 + ahead < zs:
+            take_z(s + 1 + ahead)
+        if s == 0:
+            shared_expert()
+        if s >= 2:
             combine(s - 1)
-        if s >= 2:
+        if s >= 3:
             finish(s - 2)
+    if zs > 1:
+        combine(zs - 1)
+    combine(0)
+    for s in range(max(1, zs - 2), zs):
+        finish(s)
+    finish(0)
 
     arrived(score_in, co_send.at[zs], co_recv.at[zs], sibling)
     mixed = local_sum[...] + (shared_kept[...] + score_in[...].astype(jnp.float32))
     for s in range(1, zs):
-        arrived(z_in.at[s], zo_send.at[s], zo_recv.at[s], along[s])
-        mixed = mixed + z_in[s].astype(jnp.float32)
+        arrived(z_in.at[zz[s]], zo_send.at[s], zo_recv.at[zz[s]], along[s])
+        mixed = mixed + z_in[zz[s]].astype(jnp.float32)
     local_sum[...] = mixed
     squares = jnp.sum(mixed * mixed, axis=1, keepdims=True)
     sq_out[...] = jnp.broadcast_to(squares, sq_out.shape)
@@ -251,10 +292,12 @@
     arrived(sq_in, sq_send, sq_recv, sibling)
     inverse = lax.rsqrt((squares + sq_in[:, :1]) / width + EPS)
     result_ref[...] = (
-        local_sum[...] * inverse * out_gain_ref[...].astype(jnp.float32)
+        local_sum[...] * inverse * out_gain_ref[...].astype(jnp.float32).reshape(1, half_width)
     ).astype(jnp.bfloat16)
     for copy in sent:
         copy.wait_send()
+    for copy, when in passed:
+        pl.when(when)(copy.wait_send)
 
 
 def per_device(tokens, norm_gain, routes, route_weights, gate, up, down, sgate, sup, sdown, out_gain):
@@ -295,14 +338,15 @@
             pltpu.VMEM((rows, LANES), f32),
             pltpu.VMEM((rows, LANES), f32),
             dma((6,)),
-            dma((zs,)),
-            dma((zs,)),
-            dma((zs,)),
-            dma((zs,)),
-            dma((zs,)),
-            dma((zs,)),
-            dma((zs,)),
-            dma((zs,)),
+            dma((zs, PIECES)),
+            dma((zs, PIECES)),
+            dma((zs, PIECES)),
+            dma((zs, PIECES)),
+            dma((zs, PIECES)),
+            dma((zs, PIECES)),
+            dma((zs, PIECES)),
+            dma((zs, PIECES)),
+            dma((zs, PIECES)),
             dma((zs + 1,)),
             dma((zs + 1,)),
             dma((zs,)),
@@ -320,16 +364,16 @@
         ),
     )(
         tokens,
-        norm_gain.reshape(1, -1),
-        routes,
-        route_weights,
+        norm_gain,
+        routes.T,
+        route_weights.T,
         gate,
         up,
         down,
         sgate,
         sup,
         sdown,
-        out_gain.reshape(1, -1),
+        out_gain,
     )
 
 

time: 51.2 us -> 45.1 us (0.88)
  local copies, waits for them, and re-layouts: 4.97 us -> 1.57 us
  Pallas kernels: 46 us -> 43.3 us
    pallas_call x1, Pallas kernels: 46 us -> 43.3 us  [per_device(): pl.pallas_call(functools.partial(kernel, ep), out_shape=jax.ShapeDtypeStr...]
    reshape x2 -> x0, local copies, waits for them, and re-layouts: 1.89 us -> none  [the longest x1 1.28 us: per_device(): out_gain.reshape(1, -1)]
    unnamed x9 -> x1, local copies, waits for them, and re-layouts: 3.08 us -> 1.57 us
where the time goes in v2:
time: 45.1 us; the launch traced here: 44.9 us
  Pallas kernels  43.3 us (96%)
  local copies, waits for them, and re-layouts  1.57 us (3%)
    pallas_call x1, Pallas kernels, per_device(): pl.pallas_call(functools.partial(kernel, ep), out_shape=jax.ShapeDtypeStr...  43.3 us
    unnamed x1, local copies, waits for them, and re-layouts  1.57 us

profile of v2, /device:TPU:0, one launch (start us, length us, event | category | flops | bytes accessed | tf_op | source)
XLA Modules:
  0.0 44.9 jit_solution(1137592504835929170)
XLA Ops:
  0.0 43.3 %shard_map.109 = bf16[64,1024]{1,0:T(8,128)(2,1)} custom-call(bf16[64,2048]{1,0:T(8,128)(2,1)} %tokens_ref.1, bf16[2048]{0:T(1024)(128)(2,1)} %norm_gain_ref.1, s32[4,64]{1,0:T(4,128)} %bitcast.2, f32[4,64]{1,0:T(4,128)} %bitcast.3, bf16[1,2048,256]{2,1,0:T(8,128)(2,1)} %gate_hbm.1, bf16[1,2048,256]{2,1,0:T(8,128)(2,1)} %up_hbm.1, ...), custom_call_target="tpu_custom_call" | custom-call | flops 1811939328 | bytes 6291456 | tf_op jit(solution)/shard_map/pallas_call | solution.py:314
  43.3 1.6 %copy.13 = bf16[64,1024]{1,0:T(8,128)(2,1)} copy(bf16[64,1024]{1,0:T(8,128)(2,1)} %shard_map.109) | data formatting | bytes 262144

commit v3 on v2

--- a/solution.py
+++ b/solution.py
@@ -164,7 +164,7 @@
 
     passed = []
 
-    def pass_on(block, q, source, sends, target, when):
+    def make_pass(block, q, source, sends, target, when):
         copy = pltpu.make_async_remote_copy(
             src_ref=block,
             dst_ref=block,
@@ -173,23 +173,58 @@
             device_id={"ep": target * 2 + y},
             device_id_type=MESH,
         )
-        pl.when(when)(copy.start)
         passed.append((copy, when))
+        return copy, when
 
     for q in range(PIECES):
         own = gathered.at[me, rows_of(core, q)]
-        pass_on(own, q, z, r_send, z + 1, z < zs - 1)
-        pass_on(own, q, z, l_send, z - 1, z > 0)
+        for copy, when in (
+            make_pass(own, q, z, r_send, z + 1, z < zs - 1),
+            make_pass(own, q, z, l_send, z - 1, z > 0),
+        ):
+            pl.when(when)(copy.start)
         send(own, own, y_send.at[0, q], y_recv.at[0, q], across)
 
-    def take_z(s):
+    def make(src, dst, send_sem, recv_sem, target):
+        return pltpu.make_async_remote_copy(
+            src_ref=src,
+            dst_ref=dst,
+            send_sem=send_sem,
+            recv_sem=recv_sem,
+            device_id=target,
+            device_id_type=MESH,
+        )
+
+    steps = {}
+    for s in range(1, zs):
+        steps[s] = []
         for q in range(PIECES):
             block = gathered.at[zz[s] * 2 + y, rows_of(core, q)]
-            arrived(block, r_send.at[zz[s], q], z_recv.at[zz[s], q], across)
-            pass_on(block, q, zz[s], r_send, z + 1, jnp.logical_and(zz[s] < z, z < zs - 1))
-            pass_on(block, q, zz[s], l_send, z - 1, jnp.logical_and(zz[s] > z, z > 0))
-            send(block, block, y_send.at[s, q], y_recv.at[s, q], across)
-            send(block, block, cz_send.at[s, q], cz_recv.at[s, q], sibling)
+            right = jnp.logical_and(zz[s] < z, z < zs - 1)
+            left = jnp.logical_and(zz[s] > z, z > 0)
+            passes = [
+                make_pass(block, q, zz[s], r_send, z + 1, right),
+                make_pass(block, q, zz[s], l_send, z - 1, left),
+            ]
+            coming = make(block, block, r_send.at[zz[s], q], z_recv.at[zz[s], q], across)
+            going = [
+                make(block, block, y_send.at[s, q], y_recv.at[s, q], across),
+                make(block, block, cz_send.at[s, q], cz_recv.at[s, q], sibling),
+            ]
+            sent.extend(going)
+            steps[s].append((coming, passes, going))
+
+    def take_z(s, where=None):
+        def body():
+            for coming, passes, going in steps[s]:
+                coming.wait_recv()
+                for copy, when in passes:
+                    pl.when(when)(copy.start)
+                for copy in going:
+                    copy.start()
+
+        if s < zs:
+            body() if where is None else pl.when(where)(body)
 
     def take_y(s):
         for q in range(PIECES):
@@ -255,9 +290,10 @@
         send(score_out, score_in, co_send.at[zs], co_recv.at[zs], sibling)
         shared_kept[...] = jnp.dot(act, sdown[:, my_cols], preferred_element_type=jnp.float32)
 
-    ahead = 2
-    for s in range(1, min(1 + ahead, zs)):
-        take_z(s)
+    end = jnp.logical_or(z == 0, z == zs - 1)
+    inner = jnp.logical_and(z > 0, z < zs - 1)
+    take_z(1)
+    take_z(2, inner)
     for s in range(zs):
         take_y(s)
         take_core(s)
@@ -265,18 +301,18 @@
             for i in range(3):
                 loads[i].wait()
         experts(s)
-        if s + 1 + ahead < zs:
-            take_z(s + 1 + ahead)
+        take_z(s + 3, inner)
         if s == 0:
             shared_expert()
+        take_z(s + 2, end)
+        if 1 <= s < zs - 1:
+            combine(s)
         if s >= 2:
-            combine(s - 1)
-        if s >= 3:
-            finish(s - 2)
+            finish(s - 1)
     if zs > 1:
         combine(zs - 1)
     combine(0)
-    for s in range(max(1, zs - 2), zs):
+    for s in range(max(1, zs - 1), zs):
         finish(s)
     finish(0)
 

time: 45.1 us -> 42.6 us (0.945)
  Pallas kernels: 43.3 us -> 40.9 us
    pallas_call x1, Pallas kernels: 43.3 us -> 40.9 us  [per_device(): pl.pallas_call(functools.partial(kernel, ep), out_shape=jax.ShapeDtypeStr...]
where the time goes in v3:
time: 42.6 us; the launch traced here: 42.5 us
  Pallas kernels  40.9 us (96%)
  local copies, waits for them, and re-layouts  1.57 us (4%)
    pallas_call x1, Pallas kernels, per_device(): pl.pallas_call(functools.partial(kernel, ep), out_shape=jax.ShapeDtypeStr...  40.9 us
    unnamed x1, local copies, waits for them, and re-layouts  1.57 us

profile of v3, /device:TPU:0, one launch (start us, length us, event | category | flops | bytes accessed | tf_op | source)
XLA Modules:
  0.0 42.5 jit_solution(3603507014951626377)
XLA Ops:
  0.0 40.9 %shard_map.109 = bf16[64,1024]{1,0:T(8,128)(2,1)} custom-call(bf16[64,2048]{1,0:T(8,128)(2,1)} %tokens_ref.1, bf16[2048]{0:T(1024)(128)(2,1)} %norm_gain_ref.1, s32[4,64]{1,0:T(4,128)} %bitcast.2, f32[4,64]{1,0:T(4,128)} %bitcast.3, bf16[1,2048,256]{2,1,0:T(8,128)(2,1)} %gate_hbm.1, bf16[1,2048,256]{2,1,0:T(8,128)(2,1)} %up_hbm.1, ...), custom_call_target="tpu_custom_call" | custom-call | flops 1811939328 | bytes 6291456 | tf_op jit(solution)/shard_map/pallas_call | solution.py:350
  40.9 1.6 %copy.13 = bf16[64,1024]{1,0:T(8,128)(2,1)} copy(bf16[64,1024]{1,0:T(8,128)(2,1)} %shard_map.109) | data formatting | bytes 262144
